TPU v7x, 128 devices: a whole 4x4x4 slice. The times are simulated.
128 devices in a mesh: fs: 32 (over z, y, core), tp: 4 (over x).
Axes of the slice: x: 4, y: 4, z: 4, core: 2. Of those that a mesh axis runs over, the one named last changes fastest.
Arguments:
- model_input: bfloat16 [65536, 2048], P('fs'), may hold values from -6 to 6
- value_cotan: bfloat16 [65536, 2048], P('fs', 'tp'), may hold values from -0.0234375 to 0.0234375
- mixer_cotan: bfloat16 [65536, 2048], P('fs'), may hold values from -0.0234375 to 0.0234375
- head_output: bfloat16 [65536, 2048], P('fs', 'tp'), may hold values from -6 to 6
- value_weight: float32 [2048, 2048], P('fs', 'tp'), may hold values from -0.125 to 0.125
- value_factor: bfloat16 [2048, 512], P('fs'), may hold values from -0.125 to 0.125
- value_first: float32 [512, 2048], P('fs', 'tp'), may hold values from -3 to 3
- value_second: float32 [512, 2048], P('fs', 'tp'), may hold values from 0.02 to 0.5
- output_weight: float32 [2048, 2048], P('fs', 'tp'), may hold values from -0.125 to 0.125
- output_factor: bfloat16 [2048, 512], P('fs'), may hold values from -0.125 to 0.125
- output_first: float32 [512, 2048], P('fs', 'tp'), may hold values from -3 to 3
- output_second: float32 [512, 2048], P('fs', 'tp'), may hold values from 0.02 to 0.5
Outputs:
- value_step: float32 [2048, 2048], P('fs', 'tp')
- value_updated: float32 [2048, 2048], P('fs', 'tp')
- value_first_new: float32 [512, 2048], P('fs', 'tp')
- value_second_new: float32 [512, 2048], P('fs', 'tp')
- value_copy: bfloat16 [2048, 2048], P(None, 'tp')
- output_step: float32 [2048, 2048], P('fs', 'tp')
- output_updated: float32 [2048, 2048], P('fs', 'tp')
- output_first_new: float32 [512, 2048], P('fs', 'tp')
- output_second_new: float32 [512, 2048], P('fs', 'tp')
- output_copy: bfloat16 [2048, 2048], P(None, 'tp')
All inputs are finite; a program needn't handle non-finite values.
Results may differ from a plain program's by a relative error of at most 0.0059.
Values may be sent and summed in bfloat16 or wider, within the bound.
A program may use at most 128 MiB of HBM per device.

v0:
```python
import jax
import jax.numpy as jnp
from jax import lax
from jax.sharding import Mesh
from jax.sharding import PartitionSpec as P

D = 2048
HV = 2048
FS = ("fs_0", "fs_1", "fs_2")
FS_TP = ("fs_0", "fs_1", "fs_2", "tp")


beta_first = 0.8
beta_second = 0.9
step_rate = 0.02
scale_floor = 0.25
tiny_eps = 1e-08


def sent_to_all(x, axis):
    copies = jnp.broadcast_to(x, (lax.axis_size(axis), *x.shape))
    return lax.all_to_all(copies, axis, split_axis=0, concat_axis=0, tiled=True)


def joined_along(parts, dim):
    dims = list(parts.shape[1:])
    dims[dim] *= parts.shape[0]
    return jnp.moveaxis(parts, 0, dim).reshape(dims)


def gathered_copies(x, axis, dim):
    parts = sent_to_all(x, axis)
    return joined_along(parts, dim)


def cut_along(x, dim, length):
    before, after = (x.shape[:dim], x.shape[dim + 1 :])
    return jnp.moveaxis(x.reshape(*before, length, -1, *after), dim, 0)


def sent_and_summed(x, axis, dim):
    parts = cut_along(x, dim, lax.axis_size(axis))
    arrived = lax.all_to_all(parts, axis, split_axis=0, concat_axis=0, tiled=True)
    return arrived.astype(jnp.float32).sum(axis=0)


def one_axis_at_a_time(x, axes):
    for axis in axes:
        x = lax.psum(x, axis)
    return x


def sent_together(arrays, axis, dim, along):
    ends, at = ([], 0)
    for a in arrays[:-1]:
        at += a.shape[along]
        ends.append(at)
    both = jnp.concatenate(arrays, axis=along)
    return tuple(jnp.split(lax.all_gather(both, axis, axis=dim, tiled=True), ends, axis=along))


def low_rank(rows_in, cols_in, factor, first_moment, second_moment):
    token_dims = (((0,), (0,)), ((), ()))
    reduced = jnp.dot(rows_in, gathered_copies(factor, FS, 0), preferred_element_type=jnp.float32)
    reduced_high = lax.optimization_barrier(reduced.astype(jnp.bfloat16))
    reduced_low = (reduced - reduced_high.astype(jnp.float32)).astype(jnp.bfloat16)
    high_part = lax.dot_general(
        reduced_high, cols_in, token_dims, preferred_element_type=jnp.float32
    )
    low_part = lax.dot_general(reduced_low, cols_in, token_dims, preferred_element_type=jnp.float32)
    projected = sent_and_summed((high_part + low_part).astype(jnp.bfloat16), FS, 0)
    first_new = beta_first * first_moment + (1.0 - beta_first) * projected
    second_new = beta_second * second_moment + (1.0 - beta_second) * projected * projected
    direction = (first_new / (jnp.sqrt(second_new) + tiny_eps)).astype(jnp.bfloat16)
    expanded = jnp.dot(
        factor, gathered_copies(direction, FS, 0), preferred_element_type=jnp.float32
    )
    return (expanded, first_new, second_new)


def local(
    model_input,
    value_cotan,
    mixer_cotan,
    head_output,
    value_weight,
    value_factor,
    value_first,
    value_second,
    output_weight,
    output_factor,
    output_first,
    output_second,
):
    value_exp, value_fnew, value_snew = low_rank(
        model_input, value_cotan, value_factor, value_first, value_second
    )
    output_exp, output_fnew, output_snew = low_rank(
        mixer_cotan, head_output, output_factor, output_first, output_second
    )
    value_sq, output_sq = (
        one_axis_at_a_time(jnp.sum(value_exp * value_exp), FS_TP),
        one_axis_at_a_time(jnp.sum(output_exp * output_exp), FS_TP),
    )
    value_step = step_rate / jnp.sqrt(value_sq / (D * HV) + scale_floor) * value_exp
    output_step = step_rate / jnp.sqrt(output_sq / (D * HV) + scale_floor) * output_exp
    value_updated = value_weight - value_step
    output_updated = output_weight - output_step
    value_copy, output_copy = sent_together(
        (value_updated.astype(jnp.bfloat16), output_updated.astype(jnp.bfloat16)), FS, 0, 1
    )
    return (
        value_step,
        value_updated,
        value_fnew,
        value_snew,
        value_copy,
        output_step,
        output_updated,
        output_fnew,
        output_snew,
        output_copy,
    )


def solution(mesh):
    torus = Mesh(mesh.devices.reshape(4, 4, 2, mesh.shape["tp"]), ("fs_0", "fs_1", "fs_2", "tp"))
    in_specs = (
        P(FS, None),
        P(FS, "tp"),
        P(FS, None),
        P(FS, "tp"),
        P(FS, "tp"),
        P(FS, None),
        P(FS, "tp"),
        P(FS, "tp"),
        P(FS, "tp"),
        P(FS, None),
        P(FS, "tp"),
        P(FS, "tp"),
    )
    out_specs = (
        P(FS, "tp"),
        P(FS, "tp"),
        P(FS, "tp"),
        P(FS, "tp"),
        P(None, "tp"),
        P(FS, "tp"),
        P(FS, "tp"),
        P(FS, "tp"),
        P(FS, "tp"),
        P(None, "tp"),
    )
    return jax.shard_map(local, mesh=torus, in_specs=in_specs, out_specs=out_specs, check_vma=False)
```

profile of v0, /device:TPU:1, one launch (start us, length us, event | category | flops | bytes accessed | tf_op | source)
XLA Modules:
  0.0 239.8 jit_solution(17554075201442228649)
XLA Ops:
  8.4 37.9 %all_to_all.30 = bf16[32,64,512]{2,1,0:T(8,128)(2,1)} all-to-all(bf16[32,64,512]{2,1,0:T(8,128)(2,1)S(1)} %broadcast_in_dim.12), channel_id=1, replica_groups=mesh['fs_0'=4,'fs_1'=4,'fs_2'=2,'tp'=4] {'fs_0','fs_1','fs_2'}, dimensions={0} | all-to-all | bytes 4194304 | tf_op jit(solution)/shard_map/all_to_all | solution.py:22
  46.3 1.6 broadcast_in_dim.14
  47.9 4.8 %all-to-all-start.3 = ((bf16[32,64,512]{2,1,0:T(8,128)(2,1)}), bf16[32,64,512]{2,1,0:T(8,128)(2,1)}, u32[]{:S(2)}, u32[]{:S(2)}) async-start(bf16[32,64,512]{2,1,0:T(8,128)(2,1)} %broadcast_in_dim.14), calls=%async_computation.3 | async-start | bytes 4194304 | tf_op jit(solution)/shard_map/all_to_all | solution.py:22
  52.7 7.6 %fusion.13 = (bf16[2048,512]{1,0:T(8,128)(2,1)S(1)}, f32[2048,512]{1,0:T(8,128)S(1)}) fusion(bf16[2048,2048]{1,0:T(8,128)(2,1)} %param.12, bf16[2048,512]{1,0:T(8,128)(2,1)} %bitcast.26), kind=kOutput, calls=%fused_computation.26 | convolution fusion | flops 4296015872 | bytes 16777216 | tf_op jit(solution)/shard_map/dot_general | solution.py:64
  60.2 1.3 fusion.15
  61.5 2.2 fusion.4
  63.7 17.3 %all-to-all-done.3 = bf16[32,64,512]{2,1,0:T(8,128)(2,1)} async-done(((bf16[32,64,512]{2,1,0:T(8,128)(2,1)}), bf16[32,64,512]{2,1,0:T(8,128)(2,1)}, u32[]{:S(2)}, u32[]{:S(2)}) %all-to-all-start.3) | async-done | bytes 2097184 | tf_op jit(solution)/shard_map/all_to_all | solution.py:22
  81.0 5.7 %all-to-all-start.1 = ((bf16[32,16,512]{2,1,0:T(8,128)(2,1)}), bf16[32,16,512]{2,1,0:T(8,128)(2,1)S(1)}, u32[]{:S(2)}, u32[]{:S(2)}) async-start(bf16[32,16,512]{2,1,0:T(8,128)(2,1)} %bitcast.1), calls=%async_computation.1 | async-start | bytes 1048576 | tf_op jit(solution)/shard_map/all_to_all | solution.py:43
  86.7 7.7 %fusion.14 = (bf16[2048,512]{1,0:T(8,128)(2,1)S(1)}, f32[2048,512]{1,0:T(8,128)S(1)}) fusion(bf16[2048,2048]{1,0:T(8,128)(2,1)} %param.14, bf16[2048,512]{1,0:T(8,128)(2,1)} %bitcast.4), kind=kOutput, calls=%fused_computation.27 | convolution fusion | flops 4296015872 | bytes 16777216 | tf_op jit(solution)/shard_map/dot_general | solution.py:64
  95.7 2.1 fusion.5
  98.2 7.1 %all-to-all-start.4 = ((bf16[32,16,512]{2,1,0:T(8,128)(2,1)}), bf16[32,16,512]{2,1,0:T(8,128)(2,1)S(1)}, u32[]{:S(2)}, u32[]{:S(2)}) async-start(bf16[32,16,512]{2,1,0:T(8,128)(2,1)} %bitcast.5), calls=%async_computation.4 | async-start | bytes 1048576 | tf_op jit(solution)/shard_map/all_to_all | solution.py:43
  106.1 10.7 %all-to-all-done.4 = bf16[32,16,512]{2,1,0:T(8,128)(2,1)S(1)} async-done(((bf16[32,16,512]{2,1,0:T(8,128)(2,1)}), bf16[32,16,512]{2,1,0:T(8,128)(2,1)S(1)}, u32[]{:S(2)}, u32[]{:S(2)}) %all-to-all-start.4) | async-done | bytes 524320 | tf_op jit(solution)/shard_map/all_to_all | solution.py:43
  117.6 3.9 %all-to-all-start.2 = ((bf16[32,16,512]{2,1,0:T(8,128)(2,1)}), bf16[32,16,512]{2,1,0:T(8,128)(2,1)S(1)}, u32[]{:S(2)}, u32[]{:S(2)}) async-start(bf16[32,16,512]{2,1,0:T(8,128)(2,1)} %broadcast_in_dim.13), calls=%async_computation.2 | async-start | bytes 1048576 | tf_op jit(solution)/shard_map/all_to_all | solution.py:22
  121.6 1.4 divide_convert_fusion
  123.0 10.0 %all-to-all-done.2 = bf16[32,16,512]{2,1,0:T(8,128)(2,1)S(1)} async-done(((bf16[32,16,512]{2,1,0:T(8,128)(2,1)}), bf16[32,16,512]{2,1,0:T(8,128)(2,1)S(1)}, u32[]{:S(2)}, u32[]{:S(2)}) %all-to-all-start.2) | async-done | bytes 524320 | tf_op jit(solution)/shard_map/all_to_all | solution.py:22
  133.9 3.9 %all-to-all-start.5 = ((bf16[32,16,512]{2,1,0:T(8,128)(2,1)}), bf16[32,16,512]{2,1,0:T(8,128)(2,1)S(1)}, u32[]{:S(2)}, u32[]{:S(2)}) async-start(bf16[32,16,512]{2,1,0:T(8,128)(2,1)} %broadcast_in_dim.15), calls=%async_computation.5 | async-start | bytes 1048576 | tf_op jit(solution)/shard_map/all_to_all | solution.py:22
  138.8 10.7 %all-to-all-done.5 = bf16[32,16,512]{2,1,0:T(8,128)(2,1)S(1)} async-done(((bf16[32,16,512]{2,1,0:T(8,128)(2,1)}), bf16[32,16,512]{2,1,0:T(8,128)(2,1)S(1)}, u32[]{:S(2)}, u32[]{:S(2)}) %all-to-all-start.5) | async-done | bytes 524320 | tf_op jit(solution)/shard_map/all_to_all | solution.py:22
  150.2 7.4 %all-reduce.2 = (f32[]{:T(128)}, f32[]{:T(128)}) all-reduce(f32[]{:T(128)} %get-tuple-element.34, f32[]{:T(128)} %get-tuple-element.38), channel_id=1, replica_groups=mesh['fs_0'=4,'fs_1'=4,'fs_2'=2,'tp'=4] {'fs_0'}, use_global_device_ids=true, to_apply=%region_2.0 | all-reduce | flops 2 | bytes 16 | tf_op jit(solution)/shard_map/psum | solution.py:49
  157.7 8.5 %all-reduce.1 = (f32[]{:T(128)}, f32[]{:T(128)}) all-reduce(f32[]{:T(128)} %get-tuple-element.14, f32[]{:T(128)} %get-tuple-element.15), channel_id=1, replica_groups=mesh['fs_0'=4,'fs_1'=4,'fs_2'=2,'tp'=4] {'fs_1'}, use_global_device_ids=true, to_apply=%region_3.0 | all-reduce | flops 2 | bytes 16 | tf_op jit(solution)/shard_map/psum | solution.py:49
  166.1 5.8 %all-reduce.3 = (f32[]{:T(128)}, f32[]{:T(128)}) all-reduce(f32[]{:T(128)} %get-tuple-element.12, f32[]{:T(128)} %get-tuple-element.13), channel_id=1, replica_groups=mesh['fs_0'=4,'fs_1'=4,'fs_2'=2,'tp'=4] {'fs_2'}, use_global_device_ids=true, to_apply=%region_4.0 | all-reduce | flops 2 | bytes 16 | tf_op jit(solution)/shard_map/psum | solution.py:49
  171.9 9.1 %all-reduce = (f32[]{:T(128)}, f32[]{:T(128)}) all-reduce(f32[]{:T(128)} %get-tuple-element.16, f32[]{:T(128)} %get-tuple-element.17), channel_id=1, replica_groups=mesh['fs_0'=4,'fs_1'=4,'fs_2'=2,'tp'=4] {'tp'}, use_global_device_ids=true, to_apply=%region_5.0 | all-reduce | flops 2 | bytes 16 | tf_op jit(solution)/shard_map/psum | solution.py:49
  182.4 1.7 fusion.8
  184.8 43.6 %all-gather.2.cloned.1.call-done = bf16[2048,1024]{1,0:T(8,128)(2,1)} async-done(((bf16[64,1024]{1,0:T(8,128)(2,1)}), bf16[2048,1024]{1,0:T(8,128)(2,1)}) %all-gather.2.cloned.1.call-update) | async-done | bytes 4194320 | tf_op jit(solution)/shard_map/all_gather | solution.py:59
  228.4 4.5 %fusion.12 = (bf16[2048,512]{1,0:T(8,128)(2,1)}, bf16[2048,512]{1,0:T(8,128)(2,1)}) fusion(bf16[2048,1024]{1,0:T(8,128)(2,1)} %all-gather.2.cloned.1.call-done), kind=kLoop, calls=%fused_computation.25 | loop fusion | bytes 8388608 | tf_op jit(solution)/shard_map/split | solution.py:59
  (27 shorter events, 7.9 us)
Async XLA Ops:
  7.2 53.1 %copy-start = (bf16[2048,512]{1,0:T(8,128)(2,1)S(1)}, bf16[2048,512]{1,0:T(8,128)(2,1)}, u32[]{:S(2)}) copy-start(bf16[2048,512]{1,0:T(8,128)(2,1)} %param.13) | copy-start | bytes 6291460
  8.4 37.9 %copy-start.3 = (bf16[64,512]{1,0:T(8,128)(2,1)S(1)}, bf16[64,512]{1,0:T(8,128)(2,1)}, u32[]{:S(2)}) copy-start(bf16[64,512]{1,0:T(8,128)(2,1)} %param.21) | copy-start | bytes 196612
  47.9 33.1 %all-to-all-start.3 = ((bf16[32,64,512]{2,1,0:T(8,128)(2,1)}), bf16[32,64,512]{2,1,0:T(8,128)(2,1)}, u32[]{:S(2)}, u32[]{:S(2)}) async-start(bf16[32,64,512]{2,1,0:T(8,128)(2,1)} %broadcast_in_dim.14), calls=%async_computation.3 | async-start | bytes 4194304 | tf_op jit(solution)/shard_map/all_to_all | solution.py:22
  81.0 17.2 %all-to-all-start.1 = ((bf16[32,16,512]{2,1,0:T(8,128)(2,1)}), bf16[32,16,512]{2,1,0:T(8,128)(2,1)S(1)}, u32[]{:S(2)}, u32[]{:S(2)}) async-start(bf16[32,16,512]{2,1,0:T(8,128)(2,1)} %bitcast.1), calls=%async_computation.1 | async-start | bytes 1048576 | tf_op jit(solution)/shard_map/all_to_all | solution.py:43
  86.7 7.7 %copy-start.1 = (bf16[2048,512]{1,0:T(8,128)(2,1)S(1)}, bf16[2048,512]{1,0:T(8,128)(2,1)}, u32[]{:S(2)}) copy-start(bf16[2048,512]{1,0:T(8,128)(2,1)} %param.15) | copy-start | bytes 6291460
  95.7 9.7 %copy-start.5 = (f32[16,512]{1,0:T(8,128)S(1)}, f32[16,512]{1,0:T(8,128)}, u32[]{:S(2)}) copy-start(f32[16,512]{1,0:T(8,128)} %param.19) | copy-start | bytes 98308
  95.7 9.7 %copy-start.6 = (f32[16,512]{1,0:T(8,128)S(1)}, f32[16,512]{1,0:T(8,128)}, u32[]{:S(2)}) copy-start(f32[16,512]{1,0:T(8,128)} %param.18) | copy-start | bytes 98308
  98.2 18.5 %all-to-all-start.4 = ((bf16[32,16,512]{2,1,0:T(8,128)(2,1)}), bf16[32,16,512]{2,1,0:T(8,128)(2,1)S(1)}, u32[]{:S(2)}, u32[]{:S(2)}) async-start(bf16[32,16,512]{2,1,0:T(8,128)(2,1)} %bitcast.5), calls=%async_computation.4 | async-start | bytes 1048576 | tf_op jit(solution)/shard_map/all_to_all | solution.py:43
  105.4 32.5 %copy-start.2 = (bf16[64,512]{1,0:T(8,128)(2,1)S(1)}, bf16[64,512]{1,0:T(8,128)(2,1)}, u32[]{:S(2)}) copy-start(bf16[64,512]{1,0:T(8,128)(2,1)} %param.17) | copy-start | bytes 196612
  117.6 15.5 %all-to-all-start.2 = ((bf16[32,16,512]{2,1,0:T(8,128)(2,1)}), bf16[32,16,512]{2,1,0:T(8,128)(2,1)S(1)}, u32[]{:S(2)}, u32[]{:S(2)}) async-start(bf16[32,16,512]{2,1,0:T(8,128)(2,1)} %broadcast_in_dim.13), calls=%async_computation.2 | async-start | bytes 1048576 | tf_op jit(solution)/shard_map/all_to_all | solution.py:22
  121.5 60.9 %copy-start.4 = (f32[64,512]{1,0:T(8,128)S(1)}, f32[64,512]{1,0:T(8,128)}, u32[]{:S(2)}) copy-start(f32[64,512]{1,0:T(8,128)} %param.16) | copy-start | bytes 393220
  133.9 15.5 %all-to-all-start.5 = ((bf16[32,16,512]{2,1,0:T(8,128)(2,1)}), bf16[32,16,512]{2,1,0:T(8,128)(2,1)S(1)}, u32[]{:S(2)}, u32[]{:S(2)}) async-start(bf16[32,16,512]{2,1,0:T(8,128)(2,1)} %broadcast_in_dim.15), calls=%async_computation.5 | async-start | bytes 1048576 | tf_op jit(solution)/shard_map/all_to_all | solution.py:22
  137.9 90.5 %all-gather.2.cloned.1.call-start = ((), (), s32[]{:S(2)}) async-start(), calls=%async_computation.6 | async-start | bytes 4325376 | tf_op jit(solution)/shard_map/all_gather | solution.py:59
Sparse Core Ops, SparseCore 0:
  184.9 43.4 all-gather.1
where the time goes:
time: 241 us; the launch traced here: 240 us
  waiting for transfers between devices  92.7 us (38%)
  blocking collectives  68.7 us (29%)
  starting transfers between devices  25.4 us (11%)
  matrix products  23.7 us (10%)
  between operations  15.6 us (6%)
  local copies, waits for them, and re-layouts  9.02 us (4%)
  other arithmetic  4.61 us (2%)
    all_gather x1, waiting for transfers between devices, sent_together(): lax.all_gather(both, axis, axis=dim, tiled=True)  43.6 us
    all_to_all x3, waiting for transfers between devices, sent_to_all(): return lax.all_to_all(copies, axis, split_axis=0, concat_axis=0, tiled=True)  38 us
    all_to_all x1, blocking collectives, sent_to_all(): return lax.all_to_all(copies, axis, split_axis=0, concat_axis=0, tiled=True)  37.9 us
    psum x4, blocking collectives, one_axis_at_a_time(): x = lax.psum(x, axis)  30.8 us
    dot_general x2, matrix products, low_rank(): jnp.dot(rows_in, gathered_copies(factor, FS, 0), preferred_element_type=j...  15.2 us
    all_to_all x2, starting transfers between devices, sent_and_summed(): lax.all_to_all(parts, axis, split_axis=0, concat_axis=0, tiled=True)  12.7 us
    all_to_all x3, starting transfers between devices, sent_to_all(): return lax.all_to_all(copies, axis, split_axis=0, concat_axis=0, tiled=True)  12.6 us
    all_to_all x2, waiting for transfers between devices, sent_and_summed(): lax.all_to_all(parts, axis, split_axis=0, concat_axis=0, tiled=True)  11.1 us
  transfers between devices with their start and end apart: 6, of which 6 were waited for; matrix products, arithmetic and copies ran while one was open for 10% of the time, Pallas kernels for 0%

commit v1 on v0

v1 whole, which is shorter than its diff:
```python
import functools

import jax
import jax.numpy as jnp
from jax import lax
from jax.experimental import pallas as pl
from jax.experimental.pallas import tpu as pltpu
from jax.sharding import Mesh
from jax.sharding import PartitionSpec as P

D = 2048
HV = 2048
FS = ("z", "y", "c")
MESH = pl.DeviceIdType.MESH

beta_first = 0.8
beta_second = 0.9
step_rate = 0.02
scale_floor = 0.25
tiny_eps = 1e-08

BF = jnp.bfloat16
F32 = jnp.float32


def exchange_kernel(
    rows0, cols0, rows1, cols1, w0, w1, f0, f1, a0, b0, a1, b1,
    E, W, mom, ss,
    rows, cols, colsT, gT, F, wf, mo, Pj, X, S, R, Dr, XR,
    in_sem, g_send, g_recv, d_send, d_recv, s_send, s_recv, x_send, x_recv,
):
    z, y, c, x = (lax.axis_index(n) for n in ("z", "y", "c", "x"))
    chip = z * 4 + y
    other = 1 - c
    ra = y + c * (z - y)
    rb = z + c * (y - z)

    def place(a, b):
        zz = b + c * (a - b)
        yy = a + c * (b - a)
        return zz, yy

    def shard(a, b):
        zz, yy = place(a, b)
        return (zz * 4 + yy) * 2 + c

    def at(a, b):
        zz, yy = place(a, b)
        return {"z": zz, "y": yy}

    def plus(v, k):
        return lax.rem(v + k, 4)

    def remote(src, dst, ssem, rsem, dev):
        return pltpu.make_async_remote_copy(
            src_ref=src, dst_ref=dst, send_sem=ssem, recv_sem=rsem,
            device_id=dev, device_id_type=MESH,
        )

    partner = {"c": other}

    bar = pltpu.get_barrier_semaphore()
    peers = [{"z": plus(z, k // 4), "y": plus(y, k % 4)} for k in range(1, 16)]
    xpeers = [{"x": plus(x, k)} for k in range(1, 4)]
    for p in peers + [partner] + xpeers:
        pl.semaphore_signal(bar, inc=1, device_id=p, device_id_type=MESH)

    me = chip * 2 + c
    fin = [pltpu.make_async_copy(f, F.at[m, me], in_sem.at[m]) for m, f in enumerate((f0, f1))]
    win = [pltpu.make_async_copy(w, wf.at[m], in_sem.at[2 + m]) for m, w in enumerate((w0, w1))]
    cin = [pltpu.make_async_copy(v, cols.at[m], in_sem.at[4 + m]) for m, v in enumerate((cols0, cols1))]
    rin = [
        [
            pltpu.make_async_copy(
                v.at[:, pl.ds(512 * j, 512)], rows.at[m, j], in_sem.at[6 + 4 * m + j]
            )
            for j in range(4)
        ]
        for m, v in enumerate((rows0, rows1))
    ]
    min_ = [
        pltpu.make_async_copy(v, mo.at[i], in_sem.at[14 + i]) for i, v in enumerate((a0, b0, a1, b1))
    ]
    for cp in fin + [cin[0]] + rin[0] + win + [cin[1]] + rin[1] + min_:
        cp.start()

    def G(p):
        return (F if p < 2 else W).at[p % 2]

    am, ap, af = plus(ra, 3), plus(ra, 1), plus(ra, 2)
    bm, bp, bf = plus(rb, 3), plus(rb, 1), plus(rb, 2)
    LO, HI = pl.ds(0, 32), pl.ds(32, 32)

    def send(p, s, dev, k, half=None):
        ref = G(p).at[s] if half is None else G(p).at[s, half]
        remote(ref, ref, g_send.at[p], g_recv.at[p, k], dev).start()

    def arrived(p, k, n):
        ref = G(p).at[pl.ds(0, n)]
        remote(ref, ref, g_send.at[p], g_recv.at[p, k], partner).wait_recv()

    def across(p, s):
        send(p, s, partner, 10)

    def gather_step(p, step):
        if step == 0:
            s = shard(ra, rb)
            send(p, s, at(ap, rb), 0)
            send(p, s, at(am, rb), 1)
            send(p, s, at(ra, bp), 3)
            send(p, s, at(ra, bm), 4)
            across(p, s)
        if step == 1:
            arrived(p, 0, 1)
            send(p, shard(am, rb), at(ap, rb), 2, LO)
            arrived(p, 1, 1)
            send(p, shard(ap, rb), at(am, rb), 2, HI)
            for a in (am, ap):
                send(p, shard(a, rb), at(ra, bp), 5)
                send(p, shard(a, rb), at(ra, bm), 6)
            arrived(p, 3, 1)
            send(p, shard(ra, bm), at(ra, bp), 9, LO)
            arrived(p, 4, 1)
            send(p, shard(ra, bp), at(ra, bm), 9, HI)
            for s in (shard(am, rb), shard(ap, rb), shard(ra, bm), shard(ra, bp)):
                across(p, s)
        if step == 2:
            arrived(p, 2, 1)
            send(p, shard(af, rb), at(ra, bp), 7)
            send(p, shard(af, rb), at(ra, bm), 8)
            arrived(p, 5, 2)
            for a in (am, ap):
                send(p, shard(a, bm), at(ra, bp), 9, LO)
            arrived(p, 6, 2)
            for a in (am, ap):
                send(p, shard(a, bp), at(ra, bm), 9, HI)
            across(p, shard(af, rb))
            for a in (am, ap):
                across(p, shard(a, bm))
                across(p, shard(a, bp))
        if step == 3:
            arrived(p, 7, 1)
            send(p, shard(af, bm), at(ra, bp), 9, LO)
            arrived(p, 8, 1)
            send(p, shard(af, bp), at(ra, bm), 9, HI)
            across(p, shard(af, bm))
            across(p, shard(af, bp))
        if step == 4:
            arrived(p, 9, 4)
            for a in (ra, am, ap, af):
                across(p, shard(a, bf))
        if step == 5:
            arrived(p, 10, 16)

    def gather_sent(p):
        ref = G(p).at[pl.ds(0, 31)]
        remote(ref, ref, g_send.at[p], g_recv.at[p, 0], partner).wait_send()

    def transpose_cols(m):
        cin[m].wait()
        for t in range(4):
            colsT[m, :, 512 * t : 512 * t + 512] = cols[m, 512 * t : 512 * t + 512, :].T

    def grad_chunk(m, j):
        rin[m][j].wait()
        out = jnp.dot(colsT[m], rows[m, j], preferred_element_type=F32)
        gT[m, :, 512 * j : 512 * j + 512] = out.astype(BF)

    def project(m):
        for n in range(2):
            f = F[m, :, :, 256 * n : 256 * n + 256].reshape(D, 256)
            out = jnp.dot(gT[m], f, preferred_element_type=F32)
            Pj[m, 8 * n : 8 * n + 8] = out.T.astype(BF).reshape(8, 2, 16, 512)
        remote(Pj.at[m, :, other], X.at[m], d_send.at[m], d_recv.at[m], partner).start()

    def scatter(m):
        remote(Pj.at[m, :, other], X.at[m], d_send.at[m], d_recv.at[m], partner).wait_recv()
        S[m] = (Pj[m, :, c].astype(F32) + X[m].astype(F32)).astype(BF)
        for k in (10, 9, 11, 6, 14, 2, 8, 5, 7, 13, 15, 1, 3, 4, 12):
            zz, yy = plus(z, k // 4), plus(y, k % 4)
            remote(
                S.at[m, zz * 4 + yy], R.at[m, k - 1], s_send.at[m], s_recv.at[m],
                {"z": zz, "y": yy},
            ).start()

    def moments(m):
        remote(R.at[m], R.at[m], s_send.at[m], s_recv.at[m], partner).wait_recv()
        proj = S[m, chip].astype(F32) + jnp.sum(R[m].astype(F32), axis=0)
        fnew = beta_first * mo[2 * m] + (1.0 - beta_first) * proj
        snew = beta_second * mo[2 * m + 1] + (1.0 - beta_second) * proj * proj
        mom[m, 0] = fnew
        mom[m, 1] = snew
        Dr[m, chip, c] = (fnew / (jnp.sqrt(snew) + tiny_eps)).astype(BF)
        ref = Dr.at[m, chip, c]
        for k in (10, 9, 11, 6, 14, 2, 8, 5, 7, 13, 15, 1, 3, 4, 12):
            zz, yy = plus(z, k // 4), plus(y, k % 4)
            remote(ref, ref, s_send.at[2 + m], s_recv.at[2 + m], {"z": zz, "y": yy}).start()

    def directions(m):
        remote(R.at[m], R.at[m], s_send.at[2 + m], s_recv.at[2 + m], partner).wait_recv()
        ref = Dr.at[m, :, c]
        remote(ref, ref, d_send.at[2 + m], d_recv.at[2 + m], partner).start()

    def expand(m):
        ref = Dr.at[m, :, other]
        remote(ref, ref, d_send.at[2 + m], d_recv.at[2 + m], partner).wait_recv()
        direction = Dr[m].reshape(512, 512)
        total = jnp.zeros((8, 512), F32)
        for r in range(4):
            f = F[m, 8 * r : 8 * r + 8].reshape(512, 512)
            e = jnp.dot(f, direction, preferred_element_type=F32)
            E[m, 8 * r : 8 * r + 8] = e.reshape(8, 64, 512)
            total = total + jnp.sum((e * e).reshape(64, 8, 512), axis=0)
        part = total[:, :128] + total[:, 128:256] + total[:, 256:384] + total[:, 384:]
        XR[m, x] = part
        ref = XR.at[m, x]
        for p in xpeers:
            remote(ref, ref, x_send.at[m], x_recv.at[m], p).start()

    def squares(m):
        ref = XR.at[m, pl.ds(0, 3)]
        remote(ref, ref, x_send.at[m], x_recv.at[m], partner).wait_recv()
        ss[m] = (XR[m, 0] + XR[m, 1]) + (XR[m, 2] + XR[m, 3])

    transpose_cols(0)
    fin[0].wait()
    fin[1].wait()
    grad_chunk(0, 0)
    pl.semaphore_wait(bar, 19)
    gather_step(0, 0)
    gather_step(1, 0)
    for m in range(2):
        win[m].wait()
        W[m, me] = wf[m].astype(BF)
    grad_chunk(0, 1)
    grad_chunk(0, 2)
    gather_step(0, 1)
    gather_step(1, 1)
    grad_chunk(0, 3)
    transpose_cols(1)
    grad_chunk(1, 0)
    gather_step(0, 2)
    gather_step(1, 2)
    grad_chunk(1, 1)
    grad_chunk(1, 2)
    gather_step(0, 3)
    gather_step(1, 3)
    grad_chunk(1, 3)
    gather_step(0, 4)
    gather_step(1, 4)
    gather_step(0, 5)
    project(0)
    gather_step(1, 5)
    project(1)
    scatter(0)
    gather_step(2, 0)
    gather_step(3, 0)
    scatter(1)
    for cp in min_:
        cp.wait()
    gather_step(2, 1)
    gather_step(3, 1)
    moments(0)
    gather_step(2, 2)
    gather_step(3, 2)
    moments(1)
    gather_step(2, 3)
    gather_step(3, 3)
    directions(0)
    gather_step(2, 4)
    gather_step(3, 4)
    expand(0)
    directions(1)
    expand(1)
    gather_step(2, 5)
    gather_step(3, 5)
    squares(0)
    squares(1)

    for p in range(4):
        gather_sent(p)
    for m in range(2):
        remote(X.at[m], X.at[m], d_send.at[m], d_recv.at[m], partner).wait_send()
        remote(X.at[m], X.at[m], d_send.at[2 + m], d_recv.at[2 + m], partner).wait_send()
        remote(R.at[m], R.at[m], s_send.at[m], s_recv.at[m], partner).wait_send()
        remote(R.at[m], R.at[m], s_send.at[2 + m], s_recv.at[2 + m], partner).wait_send()
        ref = XR.at[m, pl.ds(0, 3)]
        remote(ref, ref, x_send.at[m], x_recv.at[m], partner).wait_send()


def finish_kernel(
    E, W, mom, ss, w0, w1,
    step0, upd0, fn0, sn0, copy0, step1, upd1, fn1, sn1, copy1,
    wf, stage, st, up, in_sem, sem,
):
    me = (lax.axis_index("z") * 4 + lax.axis_index("y")) * 2 + lax.axis_index("c")
    win = [pltpu.make_async_copy(w, wf.at[m], in_sem.at[m]) for m, w in enumerate((w0, w1))]
    for cp in win:
        cp.start()
    done = []

    def out(src, dst):
        cp = pltpu.make_async_copy(src, dst, sem.at[len(done)])
        cp.start()
        done.append(cp)

    for m, (fn, sn) in enumerate(((fn0, sn0), (fn1, sn1))):
        out(mom.at[m, 0], fn)
        out(mom.at[m, 1], sn)
    for m, (step, upd, copy) in enumerate(((step0, upd0, copy0), (step1, upd1, copy1))):
        mean_square = jnp.sum(ss[m]) / (D * HV)
        scale = step_rate / jnp.sqrt(jnp.full((8, 512), mean_square, F32) + scale_floor)
        for r in range(4):
            e = E[m, 8 * r : 8 * r + 8].reshape(64, 8, 512)
            w = W[m, 8 * r : 8 * r + 8].reshape(512, 512).astype(F32)
            new = w - (scale[None] * e).reshape(512, 512)
            stage[m, 512 * r : 512 * r + 512] = new.astype(BF)
            out(stage.at[m, pl.ds(512 * r, 512)], copy.at[pl.ds(512 * r, 512)])
        win[m].wait()
        own = (scale[None] * E[m, me].reshape(8, 8, 512)).reshape(64, 512)
        st[m] = own
        up[m] = wf[m] - own
        out(st.at[m], step)
        out(up.at[m], upd)
    for cp in done:
        cp.wait()


def local(
    model_input, value_cotan, mixer_cotan, head_output,
    value_weight, value_factor, value_first, value_second,
    output_weight, output_factor, output_first, output_second,
):
    any_spec = pl.BlockSpec(memory_space=pl.ANY)
    vmem_spec = pl.BlockSpec(memory_space=pltpu.VMEM)
    DMA = pltpu.SemaphoreType.DMA
    E, W, mom, ss = pl.pallas_call(
        exchange_kernel,
        out_shape=(
            pltpu.VMEM((2, 32, 64, 512), F32),
            pltpu.VMEM((2, 32, 64, 512), BF),
            pltpu.VMEM((2, 2, 16, 512), F32),
            pltpu.VMEM((2, 8, 128), F32),
        ),
        in_specs=[any_spec] * 12,
        out_specs=(vmem_spec,) * 4,
        scratch_shapes=[
            pltpu.VMEM((2, 4, 2048, 512), BF),
            pltpu.VMEM((2, 2048, 512), BF),
            pltpu.VMEM((2, 512, 2048), BF),
            pltpu.VMEM((2, 512, 2048), BF),
            pltpu.VMEM((2, 32, 64, 512), BF),
            pltpu.VMEM((2, 64, 512), F32),
            pltpu.VMEM((4, 16, 512), F32),
            pltpu.VMEM((2, 16, 2, 16, 512), BF),
            pltpu.VMEM((2, 16, 16, 512), BF),
            pltpu.VMEM((2, 16, 16, 512), BF),
            pltpu.VMEM((2, 15, 16, 512), BF),
            pltpu.VMEM((2, 16, 2, 16, 512), BF),
            pltpu.VMEM((2, 4, 8, 128), F32),
            DMA((18,)),
            DMA((4,)),
            DMA((4, 11)),
            DMA((4,)),
            DMA((4,)),
            DMA((4,)),
            DMA((4,)),
            DMA((2,)),
            DMA((2,)),
        ],
        compiler_params=pltpu.CompilerParams(
            collective_id=0, has_side_effects=True, vmem_limit_bytes=44 * 1024 * 1024
        ),
        name="exchange",
    )(
        model_input, value_cotan, mixer_cotan, head_output,
        value_weight, output_weight, value_factor, output_factor,
        value_first, value_second, output_first, output_second,
    )
    shapes = []
    for _ in range(2):
        shapes += [
            jax.ShapeDtypeStruct((64, 512), F32),
            jax.ShapeDtypeStruct((64, 512), F32),
            jax.ShapeDtypeStruct((16, 512), F32),
            jax.ShapeDtypeStruct((16, 512), F32),
            jax.ShapeDtypeStruct((2048, 512), BF),
        ]
    return pl.pallas_call(
        finish_kernel,
        out_shape=tuple(shapes),
        in_specs=[vmem_spec] * 4 + [any_spec] * 2,
        out_specs=(any_spec,) * 10,
        scratch_shapes=[
            pltpu.VMEM((2, 64, 512), F32),
            pltpu.VMEM((2, 2048, 512), BF),
            pltpu.VMEM((2, 64, 512), F32),
            pltpu.VMEM((2, 64, 512), F32),
            DMA((2,)),
            DMA((16,)),
        ],
        compiler_params=pltpu.CompilerParams(vmem_limit_bytes=16 * 1024 * 1024),
        name="finish",
    )(E, W, mom, ss, value_weight, output_weight)


def solution(mesh):
    torus = Mesh(mesh.devices.reshape(4, 4, 2, mesh.shape["tp"]), ("z", "y", "c", "x"))
    rows, cols = P(FS, None), P(FS, "x")
    part = (cols, cols, cols, cols, P(None, "x"))
    return jax.shard_map(
        local, mesh=torus,
        in_specs=(rows, cols, rows, cols, cols, rows, cols, cols, cols, rows, cols, cols),
        out_specs=part + part, check_vma=False,
    )
```

time: 241 us -> 67 us (0.28)
  waiting for transfers between devices: 92.7 us -> 0 us
  blocking collectives: 68.7 us -> 0 us
  Pallas kernels: 0 us -> 66.2 us
  starting transfers between devices: 25.4 us -> 0 us
  matrix products: 23.7 us -> 0 us
  between operations: 15.6 us -> 0.69 us
  local copies, waits for them, and re-layouts: 9.02 us -> 0.01 us
  other arithmetic: 4.61 us -> 0 us
    pallas_call x0 -> x2, Pallas kernels: none -> 66.2 us  [the longest x1 62.5 us: local(): pl.pallas_call(exchange_kernel, out_shape=(pltpu.VMEM((2, 32, 64, 512), F...]
    all_to_all x5 -> x0, waiting for transfers between devices: 49.1 us -> none  [the longest x3 38 us: sent_to_all(): return lax.all_to_all(copies, axis, split_axis=0, concat_axis=0, tiled=True)]
    all_gather x1 -> x0, waiting for transfers between devices: 43.6 us -> none  [sent_together(): lax.all_gather(both, axis, axis=dim, tiled=True)]
    all_to_all x1 -> x0, blocking collectives: 37.9 us -> none  [sent_to_all(): return lax.all_to_all(copies, axis, split_axis=0, concat_axis=0, tiled=True)]
    psum x4 -> x0, blocking collectives: 30.8 us -> none  [one_axis_at_a_time(): x = lax.psum(x, axis)]
    all_to_all x5 -> x0, starting transfers between devices: 25.4 us -> none  [the longest x2 12.7 us: sent_and_summed(): lax.all_to_all(parts, axis, split_axis=0, concat_axis=0, tiled=True)]
    dot_general x8 -> x0, matrix products: 23.7 us -> none  [the longest x2 15.2 us: low_rank(): jnp.dot(rows_in, gathered_copies(factor, FS, 0), preferred_element_type=j...]
    split x1 -> x0, local copies, waits for them, and re-layouts: 4.5 us -> none  [sent_together(): jnp.split(lax.all_gather(both, axis, axis=dim, tiled=True), ends, axis=al...]
  transfers between devices with their start and end apart: 6 -> 0, of which waited for: 6 -> 0; matrix products, arithmetic and copies ran while one was open for 10% -> 0% of each run, Pallas kernels for 0% -> 0%
where the time goes in v1:
time: 67 us; the launch traced here: 66.9 us
  Pallas kernels  66.2 us (99%)
  between operations  0.69 us (1%)
    pallas_call x1, Pallas kernels, local(): pl.pallas_call(exchange_kernel, out_shape=(pltpu.VMEM((2, 32, 64, 512), F...  62.5 us
    pallas_call x1, Pallas kernels, local(): pl.pallas_call(finish_kernel, out_shape=tuple(shapes), in_specs=[vmem_spe...  3.72 us

profile of v1, /device:TPU:1, one launch (start us, length us, event | category | flops | bytes accessed | tf_op | source)
XLA Modules:
  0.0 66.9 jit_solution(10568433589693878578)
XLA Ops:
  0.6 0.0 copy-start.1
  0.7 0.0 copy-start
  0.7 62.5 %exchange.1 = (f32[2,32,64,512]{3,2,1,0:T(8,128)S(1)}, bf16[2,32,64,512]{3,2,1,0:T(8,128)(2,1)S(1)}, f32[2,2,16,512]{3,2,1,0:T(8,128)S(1)}, f32[2,8,128]{2,1,0:T(8,128)S(1)}) custom-call(bf16[2048,2048]{1,0:T(8,128)(2,1)} %rows0.1, bf16[2048,512]{1,0:T(8,128)(2,1)} %cols0.1, bf16[2048,2048]{1,0:T(8,128)(2,1)} %rows1.1, bf16[2048,512]{1,0:T(8,128)(2,1)} %cols1.1, ...), custom_call_target="tpu_custom_call" | custom-call | tf_op jit(solution)/shard_map/exchange/pallas_call | solution.py:337
  63.2 0.0 copy-done.1
  63.2 0.0 copy-done
  63.2 3.7 %finish.1 = (f32[64,512]{1,0:T(8,128)}, f32[64,512]{1,0:T(8,128)}, f32[16,512]{1,0:T(8,128)}, f32[16,512]{1,0:T(8,128)}, bf16[2048,512]{1,0:T(8,128)(2,1)}, /*in...) custom-call(f32[2,32,64,512]{3,2,1,0:T(8,128)S(1)} %get-tuple-elemen, ...), custom_call_target="tpu_custom_call" | custom-call | tf_op jit(solution)/shard_map/finish/pallas_call | solution.py:389
Async XLA Ops:
  0.6 62.5 %copy-start.1 = (f32[64,512]{1,0:T(8,128)S(1)}, f32[64,512]{1,0:T(8,128)}, u32[]{:S(2)}) copy-start(f32[64,512]{1,0:T(8,128)} %w1.3) | copy-start | bytes 393220
  0.7 62.5 %copy-start = (f32[64,512]{1,0:T(8,128)S(1)}, f32[64,512]{1,0:T(8,128)}, u32[]{:S(2)}) copy-start(f32[64,512]{1,0:T(8,128)} %w0.3) | copy-start | bytes 393220

commit v2 on v1

--- a/solution.py
+++ b/solution.py
@@ -60,7 +60,7 @@
     partner = {"c": other}
 
     bar = pltpu.get_barrier_semaphore()
-    peers = [{"z": plus(z, k // 4), "y": plus(y, k % 4)} for k in range(1, 16)]
+    peers = [{"z": plus(z, k)} for k in range(1, 4)] + [{"y": plus(y, k)} for k in range(1, 4)]
     xpeers = [{"x": plus(x, k)} for k in range(1, 4)]
     for p in peers + [partner] + xpeers:
         pl.semaphore_signal(bar, inc=1, device_id=p, device_id_type=MESH)
@@ -81,11 +81,11 @@
     min_ = [
         pltpu.make_async_copy(v, mo.at[i], in_sem.at[14 + i]) for i, v in enumerate((a0, b0, a1, b1))
     ]
-    for cp in fin + [cin[0]] + rin[0] + win + [cin[1]] + rin[1] + min_:
+    for cp in fin + [cin[0]] + win + rin[0] + [cin[1]] + rin[1] + min_:
         cp.start()
 
     def G(p):
-        return (F if p < 2 else W).at[p % 2]
+        return W.at[p - 2]
 
     am, ap, af = plus(ra, 3), plus(ra, 1), plus(ra, 2)
     bm, bp, bf = plus(rb, 3), plus(rb, 1), plus(rb, 2)
@@ -152,9 +152,78 @@
         if step == 5:
             arrived(p, 10, 16)
 
+    mine = pl.ds(32 * lax.rem(x, 2), 32)
+    xp, xm = {"x": plus(x, 1)}, {"x": plus(x, 3)}
+
+    def send_half(p, s, dev, k):
+        ref = F.at[p, s, mine]
+        remote(ref, ref, g_send.at[p], g_recv.at[p, k], dev).start()
+
+    def halves(p, k, n):
+        ref = F.at[p, pl.ds(0, n), pl.ds(0, 32)]
+        remote(ref, ref, g_send.at[p], g_recv.at[p, k], partner).wait_recv()
+
+    theirs = pl.ds(32 - 32 * lax.rem(x, 2), 32)
+
+    def over(p, s, part=None):
+        ref = F.at[p, s] if part is None else F.at[p, s, part]
+        remote(ref, ref, g_send.at[4 + p], g_recv.at[p, 10], partner).start()
+
+    def half_step(p, step):
+        if step == 0:
+            s = shard(ra, rb)
+            for k, a in ((2, af), (0, ap), (1, am)):
+                send_half(p, s, at(a, rb), k)
+            for k, b in ((5, bf), (3, bp), (4, bm)):
+                send_half(p, s, at(ra, b), k)
+            over(p, s)
+        if step == 1:
+            for k, a, dev, q in ((0, am, xp, 11), (1, ap, xm, 12), (2, af, xp, 11)):
+                halves(p, k, 1)
+                s = shard(a, rb)
+                for r, b in ((8, bf), (6, bp), (7, bm)):
+                    send_half(p, s, at(ra, b), r)
+                send_half(p, s, dev, q)
+                over(p, s, mine)
+            for k, b, dev, q in ((3, bm, xm, 12), (4, bp, xp, 11), (5, bf, xm, 12)):
+                halves(p, k, 1)
+                send_half(p, shard(ra, b), dev, q)
+                over(p, shard(ra, b), mine)
+        if step == 2:
+            for k, b, f in ((6, bm, 0), (7, bp, 1), (8, bf, 0)):
+                halves(p, k, 3)
+                for n, a in enumerate((am, ap, af)):
+                    if (n + f) % 2:
+                        send_half(p, shard(a, b), xp, 13)
+                    else:
+                        send_half(p, shard(a, b), xm, 14)
+                    over(p, shard(a, b), mine)
+        if step == 3:
+            halves(p, 11, 3)
+            for s in (shard(am, rb), shard(af, rb), shard(ra, bp)):
+                over(p, s, theirs)
+            halves(p, 12, 3)
+            for s in (shard(ap, rb), shard(ra, bm), shard(ra, bf)):
+                over(p, s, theirs)
+        if step == 4:
+            halves(p, 13, 4)
+            for s in (shard(ap, bm), shard(am, bp), shard(af, bp), shard(ap, bf)):
+                over(p, s, theirs)
+            halves(p, 14, 5)
+            for s in (shard(am, bm), shard(af, bm), shard(ap, bp), shard(am, bf), shard(af, bf)):
+                over(p, s, theirs)
+        if step == 5:
+            ref = F.at[p, pl.ds(0, 16)]
+            remote(ref, ref, g_send.at[4 + p], g_recv.at[p, 10], partner).wait_recv()
+
     def gather_sent(p):
         ref = G(p).at[pl.ds(0, 31)]
         remote(ref, ref, g_send.at[p], g_recv.at[p, 0], partner).wait_send()
+
+    def round_weights():
+        for m in range(2):
+            win[m].wait()
+            W[m, me] = wf[m].astype(BF)
 
     def transpose_cols(m):
         cin[m].wait()
@@ -165,18 +234,23 @@
         rin[m][j].wait()
         out = jnp.dot(colsT[m], rows[m, j], preferred_element_type=F32)
         gT[m, :, 512 * j : 512 * j + 512] = out.astype(BF)
+
+    def to_partner(m):
+        return remote(Pj.at[m, :, other], X.at[m], d_send.at[m], d_recv.at[m], partner)
 
     def project(m):
         for n in range(2):
             f = F[m, :, :, 256 * n : 256 * n + 256].reshape(D, 256)
             out = jnp.dot(gT[m], f, preferred_element_type=F32)
             Pj[m, 8 * n : 8 * n + 8] = out.T.astype(BF).reshape(8, 2, 16, 512)
-        remote(Pj.at[m, :, other], X.at[m], d_send.at[m], d_recv.at[m], partner).start()
+        to_partner(m).start()
+
+    FAR_FIRST = (10, 9, 11, 6, 14, 2, 8, 5, 7, 13, 15, 1, 3, 4, 12)
 
     def scatter(m):
-        remote(Pj.at[m, :, other], X.at[m], d_send.at[m], d_recv.at[m], partner).wait_recv()
+        to_partner(m).wait_recv()
         S[m] = (Pj[m, :, c].astype(F32) + X[m].astype(F32)).astype(BF)
-        for k in (10, 9, 11, 6, 14, 2, 8, 5, 7, 13, 15, 1, 3, 4, 12):
+        for k in FAR_FIRST:
             zz, yy = plus(z, k // 4), plus(y, k % 4)
             remote(
                 S.at[m, zz * 4 + yy], R.at[m, k - 1], s_send.at[m], s_recv.at[m],
@@ -184,6 +258,8 @@
             ).start()
 
     def moments(m):
+        for cp in min_[2 * m : 2 * m + 2]:
+            cp.wait()
         remote(R.at[m], R.at[m], s_send.at[m], s_recv.at[m], partner).wait_recv()
         proj = S[m, chip].astype(F32) + jnp.sum(R[m].astype(F32), axis=0)
         fnew = beta_first * mo[2 * m] + (1.0 - beta_first) * proj
@@ -192,7 +268,7 @@
         mom[m, 1] = snew
         Dr[m, chip, c] = (fnew / (jnp.sqrt(snew) + tiny_eps)).astype(BF)
         ref = Dr.at[m, chip, c]
-        for k in (10, 9, 11, 6, 14, 2, 8, 5, 7, 13, 15, 1, 3, 4, 12):
+        for k in FAR_FIRST:
             zz, yy = plus(z, k // 4), plus(y, k % 4)
             remote(ref, ref, s_send.at[2 + m], s_recv.at[2 + m], {"z": zz, "y": yy}).start()
 
@@ -222,65 +298,65 @@
         remote(ref, ref, x_send.at[m], x_recv.at[m], partner).wait_recv()
         ss[m] = (XR[m, 0] + XR[m, 1]) + (XR[m, 2] + XR[m, 3])
 
-    transpose_cols(0)
     fin[0].wait()
     fin[1].wait()
+    pl.semaphore_wait(bar, 10)
+    half_step(0, 0)
+    half_step(1, 0)
+    round_weights()
+    gather_step(2, 0)
+    transpose_cols(0)
     grad_chunk(0, 0)
-    pl.semaphore_wait(bar, 19)
-    gather_step(0, 0)
-    gather_step(1, 0)
-    for m in range(2):
-        win[m].wait()
-        W[m, me] = wf[m].astype(BF)
     grad_chunk(0, 1)
+    half_step(0, 1)
     grad_chunk(0, 2)
-    gather_step(0, 1)
-    gather_step(1, 1)
+    half_step(1, 1)
+    gather_step(3, 0)
     grad_chunk(0, 3)
+    gather_step(2, 1)
     transpose_cols(1)
     grad_chunk(1, 0)
-    gather_step(0, 2)
-    gather_step(1, 2)
+    half_step(0, 2)
     grad_chunk(1, 1)
+    half_step(1, 2)
     grad_chunk(1, 2)
-    gather_step(0, 3)
-    gather_step(1, 3)
+    half_step(0, 3)
+    gather_step(3, 1)
     grad_chunk(1, 3)
-    gather_step(0, 4)
-    gather_step(1, 4)
-    gather_step(0, 5)
+    half_step(0, 4)
+    gather_step(2, 2)
+    half_step(0, 5)
     project(0)
-    gather_step(1, 5)
+    half_step(1, 3)
+    half_step(1, 4)
+    gather_step(3, 2)
+    scatter(0)
+    half_step(1, 5)
     project(1)
-    scatter(0)
-    gather_step(2, 0)
-    gather_step(3, 0)
-    scatter(1)
-    for cp in min_:
-        cp.wait()
-    gather_step(2, 1)
-    gather_step(3, 1)
-    moments(0)
-    gather_step(2, 2)
-    gather_step(3, 2)
-    moments(1)
     gather_step(2, 3)
     gather_step(3, 3)
-    directions(0)
+    scatter(1)
+    moments(0)
+    moments(1)
     gather_step(2, 4)
     gather_step(3, 4)
+    directions(0)
+    directions(1)
     expand(0)
-    directions(1)
     expand(1)
     gather_step(2, 5)
     gather_step(3, 5)
     squares(0)
     squares(1)
 
-    for p in range(4):
-        gather_sent(p)
+    for p in range(2):
+        gather_sent(2 + p)
+        ref = F.at[p, pl.ds(0, 30), pl.ds(0, 32)]
+        remote(ref, ref, g_send.at[p], g_recv.at[p, 0], partner).wait_send()
+        ref = F.at[p, pl.ds(0, 16)]
+        remote(ref, ref, g_send.at[4 + p], g_recv.at[p, 0], partner).wait_send()
     for m in range(2):
-        remote(X.at[m], X.at[m], d_send.at[m], d_recv.at[m], partner).wait_send()
+        to_partner(m).wait_send()
         remote(X.at[m], X.at[m], d_send.at[2 + m], d_recv.at[2 + m], partner).wait_send()
         remote(R.at[m], R.at[m], s_send.at[m], s_recv.at[m], partner).wait_send()
         remote(R.at[m], R.at[m], s_send.at[2 + m], s_recv.at[2 + m], partner).wait_send()
@@ -310,12 +386,12 @@
     for m, (step, upd, copy) in enumerate(((step0, upd0, copy0), (step1, upd1, copy1))):
         mean_square = jnp.sum(ss[m]) / (D * HV)
         scale = step_rate / jnp.sqrt(jnp.full((8, 512), mean_square, F32) + scale_floor)
-        for r in range(4):
-            e = E[m, 8 * r : 8 * r + 8].reshape(64, 8, 512)
-            w = W[m, 8 * r : 8 * r + 8].reshape(512, 512).astype(F32)
-            new = w - (scale[None] * e).reshape(512, 512)
-            stage[m, 512 * r : 512 * r + 512] = new.astype(BF)
-            out(stage.at[m, pl.ds(512 * r, 512)], copy.at[pl.ds(512 * r, 512)])
+        for r in range(8):
+            e = E[m, 4 * r : 4 * r + 4].reshape(32, 8, 512)
+            w = W[m, 4 * r : 4 * r + 4].reshape(256, 512).astype(F32)
+            new = w - (scale[None] * e).reshape(256, 512)
+            stage[m, 256 * r : 256 * r + 256] = new.astype(BF)
+            out(stage.at[m, pl.ds(256 * r, 256)], copy.at[pl.ds(256 * r, 256)])
         win[m].wait()
         own = (scale[None] * E[m, me].reshape(8, 8, 512)).reshape(64, 512)
         st[m] = own
@@ -359,8 +435,8 @@
             pltpu.VMEM((2, 16, 2, 16, 512), BF),
             pltpu.VMEM((2, 4, 8, 128), F32),
             DMA((18,)),
-            DMA((4,)),
-            DMA((4, 11)),
+            DMA((6,)),
+            DMA((4, 15)),
             DMA((4,)),
             DMA((4,)),
             DMA((4,)),
@@ -397,7 +473,7 @@
             pltpu.VMEM((2, 64, 512), F32),
             pltpu.VMEM((2, 64, 512), F32),
             DMA((2,)),
-            DMA((16,)),
+            DMA((24,)),
         ],
         compiler_params=pltpu.CompilerParams(vmem_limit_bytes=16 * 1024 * 1024),
         name="finish",

time: 67 us -> 55 us (0.82)
  Pallas kernels: 66.2 us -> 54.2 us
    pallas_call x1, Pallas kernels: 62.5 us -> 50.5 us  [local(): pl.pallas_call(exchange_kernel, out_shape=(pltpu.VMEM((2, 32, 64, 512), F...]
where the time goes in v2:
time: 55 us; the launch traced here: 54.9 us
  Pallas kernels  54.2 us (99%)
  between operations  0.69 us (1%)
    pallas_call x1, Pallas kernels, local(): pl.pallas_call(exchange_kernel, out_shape=(pltpu.VMEM((2, 32, 64, 512), F...  50.5 us
    pallas_call x1, Pallas kernels, local(): pl.pallas_call(finish_kernel, out_shape=tuple(shapes), in_specs=[vmem_spe...  3.61 us

profile of v2, /device:TPU:1, one launch (start us, length us, event | category | flops | bytes accessed | tf_op | source)
XLA Modules:
  0.0 54.9 jit_solution(14557849578299981191)
XLA Ops:
  0.6 0.0 copy-start.1
  0.7 0.0 copy-start
  0.7 50.5 %exchange.1 = (f32[2,32,64,512]{3,2,1,0:T(8,128)S(1)}, bf16[2,32,64,512]{3,2,1,0:T(8,128)(2,1)S(1)}, f32[2,2,16,512]{3,2,1,0:T(8,128)S(1)}, f32[2,8,128]{2,1,0:T(8,128)S(1)}) custom-call(bf16[2048,2048]{1,0:T(8,128)(2,1)} %rows0.1, bf16[2048,512]{1,0:T(8,128)(2,1)} %cols0.1, bf16[2048,2048]{1,0:T(8,128)(2,1)} %rows1.1, bf16[2048,512]{1,0:T(8,128)(2,1)} %cols1.1, ...), custom_call_target="tpu_custom_call" | custom-call | tf_op jit(solution)/shard_map/exchange/pallas_call | solution.py:413
  51.2 0.0 copy-done.1
  51.2 0.0 copy-done
  51.2 3.6 %finish.1 = (f32[64,512]{1,0:T(8,128)}, f32[64,512]{1,0:T(8,128)}, f32[16,512]{1,0:T(8,128)}, f32[16,512]{1,0:T(8,128)}, bf16[2048,512]{1,0:T(8,128)(2,1)}, /*in...) custom-call(f32[2,32,64,512]{3,2,1,0:T(8,128)S(1)} %get-tuple-elemen, ...), custom_call_target="tpu_custom_call" | custom-call | tf_op jit(solution)/shard_map/finish/pallas_call | solution.py:465
Async XLA Ops:
  0.6 50.6 %copy-start.1 = (f32[64,512]{1,0:T(8,128)S(1)}, f32[64,512]{1,0:T(8,128)}, u32[]{:S(2)}) copy-start(f32[64,512]{1,0:T(8,128)} %w1.3) | copy-start | bytes 393220
  0.7 50.6 %copy-start = (f32[64,512]{1,0:T(8,128)S(1)}, f32[64,512]{1,0:T(8,128)}, u32[]{:S(2)}) copy-start(f32[64,512]{1,0:T(8,128)} %w0.3) | copy-start | bytes 393220

commit v3 on v2

v3 whole, which is shorter than its diff:
```python
import functools

import jax
import jax.numpy as jnp
from jax import lax
from jax.experimental import pallas as pl
from jax.experimental.pallas import tpu as pltpu
from jax.sharding import Mesh
from jax.sharding import PartitionSpec as P

D = 2048
HV = 2048
FS = ("z", "y", "c")
MESH = pl.DeviceIdType.MESH

beta_first = 0.8
beta_second = 0.9
step_rate = 0.02
scale_floor = 0.25
tiny_eps = 1e-08

BF = jnp.bfloat16
F32 = jnp.float32


def scale_of(squares):
    mean_square = jnp.sum(squares) / (D * HV)
    return step_rate / jnp.sqrt(jnp.full((8, 512), mean_square, F32) + scale_floor)


def new_step(scale, expanded):
    return (scale[None] * expanded.reshape(-1, 8, 512)).reshape(-1, 512)


def new_copy(scale, expanded, weight):
    return (weight.reshape(-1, 512).astype(F32) - new_step(scale, expanded)).astype(BF)


def exchange_kernel(
    rows0, cols0, rows1, cols1, w0, w1, f0, f1, a0, b0, a1, b1,
    E1, W, mom, ss, copy, own,
    E0, rows, cols, colsT, gT, F, wf, mo, Pj, X, S, R, Dr, XR,
    in_sem, g_send, g_recv, d_send, d_recv, s_send, s_recv, x_send, x_recv,
):
    z, y, c, x = (lax.axis_index(n) for n in ("z", "y", "c", "x"))
    chip = z * 4 + y
    other = 1 - c
    ra = y + c * (z - y)
    rb = z + c * (y - z)

    def place(a, b):
        zz = b + c * (a - b)
        yy = a + c * (b - a)
        return zz, yy

    def shard(a, b):
        zz, yy = place(a, b)
        return (zz * 4 + yy) * 2 + c

    def at(a, b):
        zz, yy = place(a, b)
        return {"z": zz, "y": yy}

    def plus(v, k):
        return lax.rem(v + k, 4)

    def remote(src, dst, ssem, rsem, dev):
        return pltpu.make_async_remote_copy(
            src_ref=src, dst_ref=dst, send_sem=ssem, recv_sem=rsem,
            device_id=dev, device_id_type=MESH,
        )

    partner = {"c": other}

    bar = pltpu.get_barrier_semaphore()
    peers = [{"z": plus(z, k)} for k in range(1, 4)] + [{"y": plus(y, k)} for k in range(1, 4)]
    xpeers = [{"x": plus(x, k)} for k in range(1, 4)]
    for p in peers + [partner] + xpeers:
        pl.semaphore_signal(bar, inc=1, device_id=p, device_id_type=MESH)

    me = chip * 2 + c
    fin = [pltpu.make_async_copy(f, F.at[m, me], in_sem.at[0]) for m, f in enumerate((f0, f1))]
    win = [pltpu.make_async_copy(w, wf.at[m], in_sem.at[1]) for m, w in enumerate((w0, w1))]
    cin = [pltpu.make_async_copy(v, cols.at[m], in_sem.at[2 + m]) for m, v in enumerate((cols0, cols1))]
    rin = [
        [
            pltpu.make_async_copy(
                v.at[:, pl.ds(512 * j, 512)], rows.at[m, j], in_sem.at[4 + 4 * m + j]
            )
            for j in range(4)
        ]
        for m, v in enumerate((rows0, rows1))
    ]
    min_ = [
        pltpu.make_async_copy(v, mo.at[i], in_sem.at[12]) for i, v in enumerate((a0, b0, a1, b1))
    ]
    for cp in fin + [cin[0]] + win + rin[0] + [cin[1]] + rin[1] + min_:
        cp.start()

    def loaded(ref, k):
        pltpu.make_async_copy(ref, ref, in_sem.at[k]).wait()

    def G(p):
        return W.at[p - 2]

    am, ap, af = plus(ra, 3), plus(ra, 1), plus(ra, 2)
    bm, bp, bf = plus(rb, 3), plus(rb, 1), plus(rb, 2)
    LO, HI = pl.ds(0, 32), pl.ds(32, 32)

    def send(p, s, dev, k, half=None):
        ref = G(p).at[s] if half is None else G(p).at[s, half]
        remote(ref, ref, g_send.at[1], g_recv.at[6 + 7 * p + k], dev).start()

    def arrived(p, k, n):
        ref = G(p).at[pl.ds(0, n)]
        remote(ref, ref, g_send.at[1], g_recv.at[6 + 7 * p + k], partner).wait_recv()

    def across(p, s):
        send(p, s, partner, 6)

    def gather_step(p, step):
        if step == 0:
            s = shard(ra, rb)
            send(p, s, at(ap, rb), 0)
            send(p, s, at(am, rb), 0)
            send(p, s, at(ra, bp), 2)
            send(p, s, at(ra, bm), 2)
            across(p, s)
        if step == 1:
            arrived(p, 0, 2)
            send(p, shard(am, rb), at(ap, rb), 1, LO)
            send(p, shard(ap, rb), at(am, rb), 1, HI)
            for a in (am, ap):
                send(p, shard(a, rb), at(ra, bp), 3)
                send(p, shard(a, rb), at(ra, bm), 3)
            arrived(p, 2, 2)
            send(p, shard(ra, bm), at(ra, bp), 5, LO)
            send(p, shard(ra, bp), at(ra, bm), 5, HI)
            for s in (shard(am, rb), shard(ap, rb), shard(ra, bm), shard(ra, bp)):
                across(p, s)
        if step == 2:
            arrived(p, 1, 1)
            send(p, shard(af, rb), at(ra, bp), 4)
            send(p, shard(af, rb), at(ra, bm), 4)
            arrived(p, 3, 4)
            for a in (am, ap):
                send(p, shard(a, bm), at(ra, bp), 5, LO)
                send(p, shard(a, bp), at(ra, bm), 5, HI)
            across(p, shard(af, rb))
            for a in (am, ap):
                across(p, shard(a, bm))
                across(p, shard(a, bp))
        if step == 3:
            arrived(p, 4, 2)
            send(p, shard(af, bm), at(ra, bp), 5, LO)
            send(p, shard(af, bp), at(ra, bm), 5, HI)
            across(p, shard(af, bm))
            across(p, shard(af, bp))
        if step == 4:
            arrived(p, 5, 4)
            for a in (ra, am, ap, af):
                across(p, shard(a, bf))
        if step == 5:
            arrived(p, 6, 16)

    mine = pl.ds(32 * lax.rem(x, 2), 32)
    xp, xm = {"x": plus(x, 1)}, {"x": plus(x, 3)}

    theirs = pl.ds(32 - 32 * lax.rem(x, 2), 32)

    def send_half(p, s, dev, k):
        ref = F.at[p, s, mine]
        remote(ref, ref, g_send.at[0], g_recv.at[10 * p + k], dev).start()

    def halves(p, k, n):
        ref = F.at[p, pl.ds(0, n), pl.ds(0, 32)]
        remote(ref, ref, g_send.at[0], g_recv.at[10 * p + k], partner).wait_recv()

    def over(p, s, part=None):
        ref = F.at[p, s] if part is None else F.at[p, s, part]
        remote(ref, ref, g_send.at[0], g_recv.at[10 * p + 7], partner).start()

    def half_step(p, step):
        if step == 0:
            s = shard(ra, rb)
            for k, a in ((2, af), (0, ap), (1, am)):
                send_half(p, s, at(a, rb), k)
            for b in (bf, bp, bm):
                send_half(p, s, at(ra, b), 3)
            over(p, s)
        if step == 1:
            for k, a, dev in ((0, am, xp), (1, ap, xm), (2, af, xp)):
                halves(p, k, 1)
                s = shard(a, rb)
                for q, b in ((6, bf), (4, bp), (5, bm)):
                    send_half(p, s, at(ra, b), q)
                send_half(p, s, dev, 8)
                over(p, s, mine)
            halves(p, 3, 3)
            for b, dev in ((bm, xm), (bp, xp), (bf, xm)):
                send_half(p, shard(ra, b), dev, 8)
                over(p, shard(ra, b), mine)
        if step == 2:
            for k, b, f in ((4, bm, 0), (5, bp, 1), (6, bf, 0)):
                halves(p, k, 3)
                for n, a in enumerate((am, ap, af)):
                    send_half(p, shard(a, b), xp if (n + f) % 2 else xm, 9)
                    over(p, shard(a, b), mine)
        if step == 3:
            halves(p, 8, 6)
            for s in [shard(a, rb) for a in (am, ap, af)] + [shard(ra, b) for b in (bm, bp, bf)]:
                over(p, s, theirs)
        if step == 4:
            halves(p, 9, 9)
            for b in (bm, bp, bf):
                for a in (am, ap, af):
                    over(p, shard(a, b), theirs)
        if step == 5:
            ref = F.at[p, pl.ds(0, 16)]
            remote(ref, ref, g_send.at[0], g_recv.at[10 * p + 7], partner).wait_recv()

    def all_sent(array, k):
        ref = array.at[:, pl.ds(0, 31)]
        remote(ref, ref, g_send.at[k], g_recv.at[0], partner).wait_send()

    def round_weights():
        loaded(wf, 1)
        for m in range(2):
            W[m, me] = wf[m].astype(BF)

    def transpose_cols(m):
        cin[m].wait()
        for t in range(4):
            colsT[m, :, 512 * t : 512 * t + 512] = cols[m, 512 * t : 512 * t + 512, :].T

    def grad_chunk(m, j):
        rin[m][j].wait()
        out = jnp.dot(colsT[m], rows[m, j], preferred_element_type=F32)
        gT[m, :, 512 * j : 512 * j + 512] = out.astype(BF)

    def to_partner(m):
        return remote(Pj.at[m, :, other], X.at[m], d_send.at[0], d_recv.at[m], partner)

    def project(m):
        for n in range(2):
            f = F[m, :, :, 256 * n : 256 * n + 256].reshape(D, 256)
            out = jnp.dot(gT[m], f, preferred_element_type=F32)
            Pj[m, 8 * n : 8 * n + 8] = out.T.astype(BF).reshape(8, 2, 16, 512)
        to_partner(m).start()

    FAR_FIRST = (10, 9, 11, 6, 14, 2, 8, 5, 7, 13, 15, 1, 3, 4, 12)

    def scatter(m):
        to_partner(m).wait_recv()
        S[m] = (Pj[m, :, c].astype(F32) + X[m].astype(F32)).astype(BF)
        for k in FAR_FIRST:
            zz, yy = plus(z, k // 4), plus(y, k % 4)
            remote(
                S.at[m, zz * 4 + yy], R.at[m, k - 1], s_send.at[0], s_recv.at[m],
                {"z": zz, "y": yy},
            ).start()

    def moments(m):
        if m == 0:
            loaded(mo, 12)
        remote(R.at[m], R.at[m], s_send.at[0], s_recv.at[m], partner).wait_recv()
        proj = S[m, chip].astype(F32) + jnp.sum(R[m].astype(F32), axis=0)
        fnew = beta_first * mo[2 * m] + (1.0 - beta_first) * proj
        snew = beta_second * mo[2 * m + 1] + (1.0 - beta_second) * proj * proj
        mom[m, 0] = fnew
        mom[m, 1] = snew
        Dr[m, chip, c] = (fnew / (jnp.sqrt(snew) + tiny_eps)).astype(BF)
        ref = Dr.at[m, chip, c]
        for k in FAR_FIRST:
            zz, yy = plus(z, k // 4), plus(y, k % 4)
            remote(ref, ref, s_send.at[1], s_recv.at[2 + m], {"z": zz, "y": yy}).start()

    def directions(m):
        remote(R.at[m], R.at[m], s_send.at[1], s_recv.at[2 + m], partner).wait_recv()
        ref = Dr.at[m, :, c]
        remote(ref, ref, d_send.at[1], d_recv.at[2 + m], partner).start()

    def expand(m):
        ref = Dr.at[m, :, other]
        remote(ref, ref, d_send.at[1], d_recv.at[2 + m], partner).wait_recv()
        direction = Dr[m].reshape(512, 512)
        total = jnp.zeros((8, 512), F32)
        for r in range(4):
            f = F[m, 8 * r : 8 * r + 8].reshape(512, 512)
            e = jnp.dot(f, direction, preferred_element_type=F32)
            (E0, E1)[m][8 * r : 8 * r + 8] = e.reshape(8, 64, 512)
            total = total + jnp.sum((e * e).reshape(64, 8, 512), axis=0)
        part = total[:, :128] + total[:, 128:256] + total[:, 256:384] + total[:, 384:]
        XR[m, x] = part
        ref = XR.at[m, x]
        for p in xpeers:
            remote(ref, ref, x_send.at[0], x_recv.at[m], p).start()

    def squares(m):
        ref = XR.at[m, pl.ds(0, 3)]
        remote(ref, ref, x_send.at[0], x_recv.at[m], partner).wait_recv()
        return (XR[m, 0] + XR[m, 1]) + (XR[m, 2] + XR[m, 3])

    def finish_first(total):
        scale = scale_of(total)
        for r in range(8):
            copy[256 * r : 256 * r + 256] = new_copy(scale, E0[4 * r : 4 * r + 4], W[0, 4 * r : 4 * r + 4])
        step = new_step(scale, E0[me])
        own[0] = step
        own[1] = wf[0] - step

    loaded(F.at[:, me], 0)
    pl.semaphore_wait(bar, 10)
    half_step(0, 0)
    half_step(1, 0)
    transpose_cols(0)
    round_weights()
    gather_step(2, 0)
    grad_chunk(0, 0)
    grad_chunk(0, 1)
    half_step(0, 1)
    grad_chunk(0, 2)
    half_step(1, 1)
    gather_step(3, 0)
    grad_chunk(0, 3)
    gather_step(2, 1)
    transpose_cols(1)
    grad_chunk(1, 0)
    half_step(0, 2)
    grad_chunk(1, 1)
    half_step(1, 2)
    half_step(0, 3)
    grad_chunk(1, 2)
    gather_step(3, 1)
    grad_chunk(1, 3)
    half_step(0, 4)
    gather_step(2, 2)
    half_step(1, 3)
    half_step(0, 5)
    project(0)
    half_step(1, 4)
    scatter(0)
    half_step(1, 5)
    project(1)
    scatter(1)
    moments(0)
    moments(1)
    gather_step(2, 3)
    gather_step(3, 2)
    directions(0)
    expand(0)
    directions(1)
    gather_step(2, 4)
    gather_step(3, 3)
    expand(1)
    gather_step(2, 5)
    finish_first(squares(0))
    gather_step(3, 4)
    ss[...] = squares(1)
    gather_step(3, 5)

    all_sent(F, 0)
    all_sent(W, 1)
    for k in range(2):
        remote(X, X, d_send.at[k], d_recv.at[0], partner).wait_send()
        remote(R, R, s_send.at[k], s_recv.at[0], partner).wait_send()
    ref = XR.at[:, pl.ds(0, 3)]
    remote(ref, ref, x_send.at[0], x_recv.at[0], partner).wait_send()


def finish_kernel(
    E, W, mom, ss, copy_first, own_first, w1,
    step0, upd0, fn0, sn0, copy0, step1, upd1, fn1, sn1, copy1,
    wf, stage, st, up, in_sem, sem,
):
    me = (lax.axis_index("z") * 4 + lax.axis_index("y")) * 2 + lax.axis_index("c")
    win = pltpu.make_async_copy(w1, wf, in_sem)
    win.start()
    done = []

    def out(src, dst):
        cp = pltpu.make_async_copy(src, dst, sem.at[len(done)])
        cp.start()
        done.append(cp)

    for q in range(2):
        out(copy_first.at[pl.ds(1024 * q, 1024)], copy0.at[pl.ds(1024 * q, 1024)])
    out(own_first.at[0], step0)
    out(own_first.at[1], upd0)
    for m, (fn, sn) in enumerate(((fn0, sn0), (fn1, sn1))):
        out(mom.at[m, 0], fn)
        out(mom.at[m, 1], sn)
    scale = scale_of(ss[...])
    for r in range(8):
        stage[256 * r : 256 * r + 256] = new_copy(scale, E[4 * r : 4 * r + 4], W[1, 4 * r : 4 * r + 4])
        out(stage.at[pl.ds(256 * r, 256)], copy1.at[pl.ds(256 * r, 256)])
    step = new_step(scale, E[me])
    st[...] = step
    out(st, step1)
    win.wait()
    up[...] = wf[...] - step
    out(up, upd1)
    for cp in done:
        cp.wait()


def local(
    model_input, value_cotan, mixer_cotan, head_output,
    value_weight, value_factor, value_first, value_second,
    output_weight, output_factor, output_first, output_second,
):
    any_spec = pl.BlockSpec(memory_space=pl.ANY)
    vmem_spec = pl.BlockSpec(memory_space=pltpu.VMEM)
    DMA = pltpu.SemaphoreType.DMA
    results = pl.pallas_call(
        exchange_kernel,
        out_shape=(
            pltpu.VMEM((32, 64, 512), F32),
            pltpu.VMEM((2, 32, 64, 512), BF),
            pltpu.VMEM((2, 2, 16, 512), F32),
            pltpu.VMEM((8, 128), F32),
            pltpu.VMEM((2048, 512), BF),
            pltpu.VMEM((2, 64, 512), F32),
        ),
        in_specs=[any_spec] * 12,
        out_specs=(vmem_spec,) * 6,
        scratch_shapes=[
            pltpu.VMEM((32, 64, 512), F32),
            pltpu.VMEM((2, 4, 2048, 512), BF),
            pltpu.VMEM((2, 2048, 512), BF),
            pltpu.VMEM((2, 512, 2048), BF),
            pltpu.VMEM((2, 512, 2048), BF),
            pltpu.VMEM((2, 32, 64, 512), BF),
            pltpu.VMEM((2, 64, 512), F32),
            pltpu.VMEM((4, 16, 512), F32),
            pltpu.VMEM((2, 16, 2, 16, 512), BF),
            pltpu.VMEM((2, 16, 16, 512), BF),
            pltpu.VMEM((2, 16, 16, 512), BF),
            pltpu.VMEM((2, 15, 16, 512), BF),
            pltpu.VMEM((2, 16, 2, 16, 512), BF),
            pltpu.VMEM((2, 4, 8, 128), F32),
            DMA((13,)),
            DMA((2,)),
            DMA((34,)),
            DMA((2,)),
            DMA((4,)),
            DMA((2,)),
            DMA((4,)),
            DMA((1,)),
            DMA((2,)),
        ],
        compiler_params=pltpu.CompilerParams(
            collective_id=0, has_side_effects=True, vmem_limit_bytes=44 * 1024 * 1024
        ),
        name="exchange",
    )(
        model_input, value_cotan, mixer_cotan, head_output,
        value_weight, output_weight, value_factor, output_factor,
        value_first, value_second, output_first, output_second,
    )
    shapes = []
    for _ in range(2):
        shapes += [
            jax.ShapeDtypeStruct((64, 512), F32),
            jax.ShapeDtypeStruct((64, 512), F32),
            jax.ShapeDtypeStruct((16, 512), F32),
            jax.ShapeDtypeStruct((16, 512), F32),
            jax.ShapeDtypeStruct((2048, 512), BF),
        ]
    return pl.pallas_call(
        finish_kernel,
        out_shape=tuple(shapes),
        in_specs=[vmem_spec] * 6 + [any_spec],
        out_specs=(any_spec,) * 10,
        scratch_shapes=[
            pltpu.VMEM((64, 512), F32),
            pltpu.VMEM((2048, 512), BF),
            pltpu.VMEM((64, 512), F32),
            pltpu.VMEM((64, 512), F32),
            DMA,
            DMA((18,)),
        ],
        compiler_params=pltpu.CompilerParams(vmem_limit_bytes=8 * 1024 * 1024),
        name="finish",
    )(*results, output_weight)


def solution(mesh):
    torus = Mesh(mesh.devices.reshape(4, 4, 2, mesh.shape["tp"]), ("z", "y", "c", "x"))
    rows, cols = P(FS, None), P(FS, "x")
    part = (cols, cols, cols, cols, P(None, "x"))
    return jax.shard_map(
        local, mesh=torus,
        in_specs=(rows, cols, rows, cols, cols, rows, cols, cols, cols, rows, cols, cols),
        out_specs=part + part, check_vma=False,
    )
```

time: 55 us -> 51.3 us (0.933)
  Pallas kernels: 54.2 us -> 50.5 us
    pallas_call x1, Pallas kernels: 50.5 us -> 47.9 us  [local(): pl.pallas_call(exchange_kernel, out_shape=(pltpu.VMEM((32, 64, 512), F32)...]
    pallas_call x1, Pallas kernels: 3.61 us -> 2.55 us  [local(): pl.pallas_call(finish_kernel, out_shape=tuple(shapes), in_specs=[vmem_spe...]
where the time goes in v3:
time: 51.3 us; the launch traced here: 51.2 us
  Pallas kernels  50.5 us (98%)
  between operations  0.67 us (1%)
    pallas_call x1, Pallas kernels, local(): pl.pallas_call(exchange_kernel, out_shape=(pltpu.VMEM((32, 64, 512), F32)...  47.9 us
    pallas_call x1, Pallas kernels, local(): pl.pallas_call(finish_kernel, out_shape=tuple(shapes), in_specs=[vmem_spe...  2.55 us

profile of v3, /device:TPU:1, one launch (start us, length us, event | category | flops | bytes accessed | tf_op | source)
XLA Modules:
  0.0 51.2 jit_solution(16618984629327430456)
XLA Ops:
  0.6 0.0 copy-start
  0.7 47.9 %exchange.1 = (f32[32,64,512]{2,1,0:T(8,128)S(1)}, bf16[2,32,64,512]{3,2,1,0:T(8,128)(2,1)S(1)}, f32[2,2,16,512]{3,2,1,0:T(8,128)S(1)}, f32[8,128]{1,0:T(8,128)S...) custom-call(bf16[2048,2048]{1,0:T(8,128)(2,1)} %rows0.1, bf16[2048,512]{1,0:T(8,128)(2,1)} %cols0.1, ...), custom_call_target="tpu_custom_call" | custom-call | tf_op jit(solution)/shard_map/exchange/pallas_call | solution.py:415
  48.6 0.0 copy-done
  48.6 2.5 %finish.1 = (f32[64,512]{1,0:T(8,128)}, f32[64,512]{1,0:T(8,128)}, f32[16,512]{1,0:T(8,128)}, f32[16,512]{1,0:T(8,128)}, bf16[2048,512]{1,0:T(8,128)(2,1)}, /*in...) custom-call(f32[32,64,512]{2,1,0:T(8,128)S(1)} %get-tuple-element.16, ...), custom_call_target="tpu_custom_call" | custom-call | tf_op jit(solution)/shard_map/finish/pallas_call | solution.py:470
Async XLA Ops:
  0.6 48.0 %copy-start = (f32[64,512]{1,0:T(8,128)S(1)}, f32[64,512]{1,0:T(8,128)}, u32[]{:S(2)}) copy-start(f32[64,512]{1,0:T(8,128)} %w1.3) | copy-start | bytes 393220

commit v4 on v3

--- a/solution.py
+++ b/solution.py
@@ -85,16 +85,16 @@
     rin = [
         [
             pltpu.make_async_copy(
-                v.at[:, pl.ds(512 * j, 512)], rows.at[m, j], in_sem.at[4 + 4 * m + j]
+                v.at[:, pl.ds(512 * j, 512)], rows.at[m, j], in_sem.at[4 + j]
             )
             for j in range(4)
         ]
         for m, v in enumerate((rows0, rows1))
     ]
     min_ = [
-        pltpu.make_async_copy(v, mo.at[i], in_sem.at[12]) for i, v in enumerate((a0, b0, a1, b1))
+        pltpu.make_async_copy(v, mo.at[i], in_sem.at[8]) for i, v in enumerate((a0, b0, a1, b1))
     ]
-    for cp in fin + [cin[0]] + win + rin[0] + [cin[1]] + rin[1] + min_:
+    for cp in fin + [cin[0]] + win + rin[0] + [cin[1]] + min_:
         cp.start()
 
     def loaded(ref, k):
@@ -235,6 +235,8 @@
 
     def grad_chunk(m, j):
         rin[m][j].wait()
+        if m == 0:
+            rin[1][j].start()
         out = jnp.dot(colsT[m], rows[m, j], preferred_element_type=F32)
         gT[m, :, 512 * j : 512 * j + 512] = out.astype(BF)
 
@@ -262,7 +264,7 @@
 
     def moments(m):
         if m == 0:
-            loaded(mo, 12)
+            loaded(mo, 8)
         remote(R.at[m], R.at[m], s_send.at[0], s_recv.at[m], partner).wait_recv()
         proj = S[m, chip].astype(F32) + jnp.sum(R[m].astype(F32), axis=0)
         fnew = beta_first * mo[2 * m] + (1.0 - beta_first) * proj
@@ -332,9 +334,9 @@
     half_step(0, 3)
     grad_chunk(1, 2)
     gather_step(3, 1)
+    gather_step(2, 2)
     grad_chunk(1, 3)
     half_step(0, 4)
-    gather_step(2, 2)
     half_step(1, 3)
     half_step(0, 5)
     project(0)
@@ -343,9 +345,9 @@
     half_step(1, 5)
     project(1)
     scatter(1)
+    gather_step(2, 3)
     moments(0)
     moments(1)
-    gather_step(2, 3)
     gather_step(3, 2)
     directions(0)
     expand(0)
@@ -371,37 +373,33 @@
 def finish_kernel(
     E, W, mom, ss, copy_first, own_first, w1,
     step0, upd0, fn0, sn0, copy0, step1, upd1, fn1, sn1, copy1,
-    wf, stage, st, up, in_sem, sem,
+    wf, stage, st, in_sem, sem,
 ):
     me = (lax.axis_index("z") * 4 + lax.axis_index("y")) * 2 + lax.axis_index("c")
     win = pltpu.make_async_copy(w1, wf, in_sem)
     win.start()
-    done = []
-
-    def out(src, dst):
-        cp = pltpu.make_async_copy(src, dst, sem.at[len(done)])
-        cp.start()
-        done.append(cp)
-
-    for q in range(2):
-        out(copy_first.at[pl.ds(1024 * q, 1024)], copy0.at[pl.ds(1024 * q, 1024)])
-    out(own_first.at[0], step0)
-    out(own_first.at[1], upd0)
+
+    def out(src, dst, k):
+        pltpu.make_async_copy(src, dst, sem.at[k]).start()
+
+    out(copy_first, copy0, 0)
+    out(own_first.at[0], step0, 1)
+    out(own_first.at[1], upd0, 1)
     for m, (fn, sn) in enumerate(((fn0, sn0), (fn1, sn1))):
-        out(mom.at[m, 0], fn)
-        out(mom.at[m, 1], sn)
+        out(mom.at[m, 0], fn, 2)
+        out(mom.at[m, 1], sn, 2)
     scale = scale_of(ss[...])
     for r in range(8):
         stage[256 * r : 256 * r + 256] = new_copy(scale, E[4 * r : 4 * r + 4], W[1, 4 * r : 4 * r + 4])
-        out(stage.at[pl.ds(256 * r, 256)], copy1.at[pl.ds(256 * r, 256)])
+        out(stage.at[pl.ds(256 * r, 256)], copy1.at[pl.ds(256 * r, 256)], 3)
     step = new_step(scale, E[me])
-    st[...] = step
-    out(st, step1)
+    st[0] = step
+    out(st.at[0], step1, 4)
     win.wait()
-    up[...] = wf[...] - step
-    out(up, upd1)
-    for cp in done:
-        cp.wait()
+    st[1] = wf[...] - step
+    out(st.at[1], upd1, 4)
+    for k, ref in enumerate((copy_first, own_first, mom, stage, st)):
+        pltpu.make_async_copy(ref, ref, sem.at[k]).wait()
 
 
 def local(
@@ -439,7 +437,7 @@
             pltpu.VMEM((2, 15, 16, 512), BF),
             pltpu.VMEM((2, 16, 2, 16, 512), BF),
             pltpu.VMEM((2, 4, 8, 128), F32),
-            DMA((13,)),
+            DMA((9,)),
             DMA((2,)),
             DMA((34,)),
             DMA((2,)),
@@ -475,10 +473,9 @@
         scratch_shapes=[
             pltpu.VMEM((64, 512), F32),
             pltpu.VMEM((2048, 512), BF),
-            pltpu.VMEM((64, 512), F32),
-            pltpu.VMEM((64, 512), F32),
+            pltpu.VMEM((2, 64, 512), F32),
             DMA,
-            DMA((18,)),
+            DMA((5,)),
         ],
         compiler_params=pltpu.CompilerParams(vmem_limit_bytes=8 * 1024 * 1024),
         name="finish",

time: 51.3 us -> 51.2 us (level)
  no operation moved by 1% of the time
where the time goes in v4:
time: 51.2 us; the launch traced here: 51 us
  Pallas kernels  50.3 us (98%)
  between operations  0.67 us (1%)
    pallas_call x1, Pallas kernels, local(): pl.pallas_call(exchange_kernel, out_shape=(pltpu.VMEM((32, 64, 512), F32)...  47.9 us
    pallas_call x1, Pallas kernels, local(): pl.pallas_call(finish_kernel, out_shape=tuple(shapes), in_specs=[vmem_spe...  2.43 us

profile of v4, /device:TPU:1, one launch (start us, length us, event | category | flops | bytes accessed | tf_op | source)
XLA Modules:
  0.0 51.0 jit_solution(14656935398498793657)
XLA Ops:
  0.6 0.0 copy-start
  0.7 47.9 %exchange.1 = (f32[32,64,512]{2,1,0:T(8,128)S(1)}, bf16[2,32,64,512]{3,2,1,0:T(8,128)(2,1)S(1)}, f32[2,2,16,512]{3,2,1,0:T(8,128)S(1)}, f32[8,128]{1,0:T(8,128)S...) custom-call(bf16[2048,2048]{1,0:T(8,128)(2,1)} %rows0.1, bf16[2048,512]{1,0:T(8,128)(2,1)} %cols0.1, ...), custom_call_target="tpu_custom_call" | custom-call | tf_op jit(solution)/shard_map/exchange/pallas_call | solution.py:413
  48.5 0.0 copy-done
  48.5 2.4 %finish.1 = (f32[64,512]{1,0:T(8,128)}, f32[64,512]{1,0:T(8,128)}, f32[16,512]{1,0:T(8,128)}, f32[16,512]{1,0:T(8,128)}, bf16[2048,512]{1,0:T(8,128)(2,1)}, /*in...) custom-call(f32[32,64,512]{2,1,0:T(8,128)S(1)} %get-tuple-element.16, ...), custom_call_target="tpu_custom_call" | custom-call | tf_op jit(solution)/shard_map/finish/pallas_call | solution.py:468
Async XLA Ops:
  0.6 47.9 %copy-start = (f32[64,512]{1,0:T(8,128)S(1)}, f32[64,512]{1,0:T(8,128)}, u32[]{:S(2)}) copy-start(f32[64,512]{1,0:T(8,128)} %w1.3) | copy-start | bytes 393220
